TPU v7x, 32 devices: a whole 2x2x4 slice. The times are simulated.
32 devices in a mesh: grp: 2 (over y), dp: 2 (over x), kv: 4 (over z), tp: 2 (over core).
Axes of the slice: x: 2, y: 2, z: 4, core: 2. Of those that a mesh axis runs over, the one named last changes fastest.
Arguments:
- inputs: bfloat16 [32, 4096], P(('grp', 'dp'), 'kv'), parts along dimension 0, may hold values from -6 to 6
- gain_in: float32 [4096], P('kv'), may hold values from 0.1 to 1.9
- w_gate: bfloat16 [4096, 2048], P('kv', 'tp'), may hold values from -0.09375 to 0.09375
- w_input: bfloat16 [4096, 2048], P('kv', 'tp'), may hold values from -0.09375 to 0.09375
- w_bproj: bfloat16 [4096, 1024], P('kv', 'tp'), may hold values from -0.09375 to 0.09375
- w_cproj: bfloat16 [4096, 1024], P('kv', 'tp'), may hold values from -0.09375 to 0.09375
- w_step: bfloat16 [4096, 32], P('kv', 'tp'), may hold values from -0.09375 to 0.09375
- conv_input: float32 [4, 2048], P(None, 'tp'), may hold values from -3 to 3
- conv_bproj: float32 [4, 1024], P(None, 'tp'), may hold values from -3 to 3
- conv_cproj: float32 [4, 1024], P(None, 'tp'), may hold values from -3 to 3
- tail_input: bfloat16 [32, 3, 2048], P(('grp', 'dp', 'kv'), None, 'tp'), parts along dimension 0, may hold values from -6 to 6
- tail_bproj: bfloat16 [32, 3, 1024], P(('grp', 'dp', 'kv'), None, 'tp'), parts along dimension 0, may hold values from -6 to 6
- tail_cproj: bfloat16 [32, 3, 1024], P(('grp', 'dp', 'kv'), None, 'tp'), parts along dimension 0, may hold values from -6 to 6
- step_bias: float32 [32], P('tp'), may hold values from -3 to 0
- decay_log: float32 [32], P('tp'), may hold values from -2 to 2
- block_input: bfloat16 [32, 128, 2048], P(('grp', 'dp', 'kv'), None, 'tp'), parts along dimension 0, may hold values from -6 to 6
- block_bproj: bfloat16 [32, 128, 1024], P(('grp', 'dp', 'kv'), None, 'tp'), parts along dimension 0, may hold values from -0.59765625 to 0.59765625
- block_step: float32 [32, 128, 32], P(('grp', 'dp', 'kv'), None, 'tp'), parts along dimension 0, may hold values from 0.005 to 0.2
- lengths: int32 [32], P(('grp', 'dp', 'kv')), parts along dimension 0, may hold values from 1 to 127, 512 in all
- state: float32 [32, 32, 64, 128], P(('grp', 'dp', 'kv'), 'tp'), parts along dimension 0, may hold values from -0.6 to 0.6
- gain_mix: float32 [2048], P('tp'), may hold values from 0.1 to 1.9
- w_out: bfloat16 [2048, 4096], P('tp', 'kv'), may hold values from -0.125 to 0.125
- gain_mlp: float32 [4096], P(('kv', 'tp')), may hold values from 0.1 to 1.9
- w_up: bfloat16 [4096, 16384], P(('kv', 'tp'), 'dp'), may hold values from -0.09375 to 0.09375
- w_down: bfloat16 [16384, 4096], P('dp', ('kv', 'tp')), may hold values from -0.046875 to 0.046875
Outputs:
- layer_out: bfloat16 [32, 4096], P(('grp', 'dp'), ('kv', 'tp')), parts along dimension 0
There are 2 independent parts, one for each index of `grp`. A program takes and returns all parts, laid end to end along the dimension named above; an argument that names none is the same for every part. Nothing has to cross between parts.
Inputs may be any that keep to these rules, and one draw needn't show every extreme that they name: `lengths`: the number of live positions before the new token in each sequence's current block; the largest equals 127 in every draw.
All inputs are finite; a program needn't handle non-finite values.
Results may differ from a plain program's by a relative error of at most 0.012.
Values may be sent and summed in bfloat16 or wider, within the bound.
A program may use at most 64 MiB of HBM per device.

v0:
```python
import jax
import jax.numpy as jnp
from jax import lax
from jax.sharding import PartitionSpec as P

D = 4096
HEAD_DIM = 64
D_STATE = 128
TAPS = 4
SSM_WIDTH = 2048
EPS = 1e-06


def convolve(history, weights, newest):
    summed = weights[TAPS - 1] * newest
    for offset in range(TAPS - 1):
        summed = summed + weights[offset] * history[:, offset].astype(jnp.float32)
    return jax.nn.silu(summed)


def per_device(
    inputs,
    gain_in,
    w_gate,
    w_input,
    w_bproj,
    w_cproj,
    w_step,
    conv_input,
    conv_bproj,
    conv_cproj,
    tail_input,
    tail_bproj,
    tail_cproj,
    step_bias,
    decay_log,
    block_input,
    block_bproj,
    block_step,
    lengths,
    state,
    gain_mix,
    w_out,
    gain_mlp,
    w_up,
    w_down,
):
    stream = inputs.astype(jnp.float32)
    squares = jnp.sum(stream * stream, axis=1)
    scaled = (stream * gain_in).astype(jnp.bfloat16)
    matrices = (w_gate, w_input, w_bproj, w_cproj, w_step)
    pieces = [jnp.dot(scaled, weight, preferred_element_type=jnp.float32) for weight in matrices]
    projected, totals = (
        lax.psum_scatter(jnp.concatenate(pieces, axis=1), "kv", scatter_dimension=0, tiled=True),
        lax.psum_scatter(squares, "kv", scatter_dimension=0, tiled=True),
    )
    inverse = lax.rsqrt(totals / D + EPS)[:, None]
    bounds = [0]
    for weight in matrices:
        bounds.append(bounds[-1] + weight.shape[1])
    gate_pre, value_pre, b_pre, c_pre, step_pre = [
        projected[:, bounds[member] : bounds[member + 1]] * inverse for member in range(5)
    ]
    seq_count = lengths.shape[0]
    head_count = step_bias.shape[0]
    group_count = w_bproj.shape[1] // D_STATE
    block_len = block_step.shape[1]
    per_group = head_count // group_count
    current = convolve(tail_input, conv_input, value_pre)
    b_now = convolve(tail_bproj, conv_bproj, b_pre)
    c_now = convolve(tail_cproj, conv_cproj, c_pre)
    step_size = jax.nn.softplus(step_pre + step_bias)
    decay_rate = -jnp.exp(decay_log)
    positions = lax.broadcasted_iota(jnp.int32, (1, block_len), 1)
    live_rows = (positions < lengths[:, None]).astype(jnp.float32)
    masked = block_step * live_rows[:, :, None]
    later_steps = jnp.sum(masked, axis=1, keepdims=True) - jnp.cumsum(masked, axis=1)
    decays = jnp.exp(decay_rate * (step_size[:, None, :] + later_steps)) * live_rows[:, :, None]
    c_query = c_now.astype(jnp.bfloat16).reshape(seq_count, group_count, D_STATE)
    keys = block_bproj.reshape(seq_count, block_len, group_count, D_STATE)
    scores = jnp.einsum("bsgn,bgn->bsg", keys, c_query, preferred_element_type=jnp.float32)
    scores = jnp.repeat(scores, per_group, axis=2)
    weights = (decays * scores * block_step).astype(jnp.bfloat16)
    values = block_input.reshape(seq_count, block_len, head_count, HEAD_DIM)
    inner_sum = jnp.einsum("bsh,bshp->bhp", weights, values, preferred_element_type=jnp.float32)
    c_full = c_now.reshape(seq_count, group_count, D_STATE)
    b_full = b_now.reshape(seq_count, group_count, D_STATE)
    own_score = jnp.repeat(jnp.sum(c_full * b_full, axis=2), per_group, axis=1)
    own_term = (step_size * own_score)[:, :, None] * current.reshape(
        seq_count, head_count, HEAD_DIM
    )
    carried = jnp.exp(decay_rate * (step_size + jnp.sum(masked, axis=1)))
    c_heads = jnp.repeat(c_full, per_group, axis=1)
    readout = jnp.einsum("bhpn,bhn->bhp", state, c_heads, precision=lax.Precision.HIGHEST)
    mixed = (inner_sum + own_term + carried[:, :, None] * readout).reshape(
        seq_count, -1
    ) * jax.nn.silu(gate_pre)
    local_sq = jnp.sum(mixed * mixed, axis=1)
    total_sq = lax.psum(local_sq, "tp")
    normed = (mixed * lax.rsqrt(total_sq / SSM_WIDTH + EPS)[:, None] * gain_mix).astype(
        jnp.bfloat16
    )
    products = jnp.dot(
        lax.all_gather(normed, "kv", axis=0, tiled=True), w_out, preferred_element_type=jnp.float32
    )
    mixed_in = lax.psum_scatter(products, "tp", scatter_dimension=1, tiled=True)
    column_count = mixed_in.shape[1]
    residual = lax.dynamic_slice_in_dim(
        stream, lax.axis_index("tp") * column_count, column_count, 1
    )
    hidden = (residual + mixed_in).astype(jnp.bfloat16)
    lifted = (hidden.astype(jnp.float32) * gain_mlp).astype(jnp.bfloat16)
    all_lifted, all_hidden = (
        lax.all_gather(lifted, "dp", axis=0, tiled=True),
        lax.all_gather(hidden, "dp", axis=0, tiled=True),
    )
    whole_rows = all_hidden.astype(jnp.float32)
    row_sq = jnp.sum(whole_rows * whole_rows, axis=1)
    partial_value = jnp.dot(all_lifted, w_up, preferred_element_type=jnp.float32)
    sq_sum = lax.psum(row_sq, ("kv", "tp"))
    shares = lax.psum_scatter(partial_value, ("kv", "tp"), scatter_dimension=1, tiled=True)
    unit_share = jnp.square(jax.nn.relu(shares * lax.rsqrt(sq_sum / D + EPS)[:, None])).astype(
        jnp.bfloat16
    )
    hidden_units = lax.all_gather(unit_share, ("kv", "tp"), axis=1, tiled=True)
    lowered = lax.psum_scatter(
        jnp.dot(hidden_units, w_down, preferred_element_type=jnp.float32),
        "dp",
        scatter_dimension=0,
        tiled=True,
    )
    return (hidden.astype(jnp.float32) + lowered).astype(jnp.bfloat16)


def solution(mesh):
    return jax.shard_map(
        per_device,
        mesh=mesh,
        in_specs=(
            P(("grp", "dp"), "kv"),
            P("kv"),
            P("kv", "tp"),
            P("kv", "tp"),
            P("kv", "tp"),
            P("kv", "tp"),
            P("kv", "tp"),
            P(None, "tp"),
            P(None, "tp"),
            P(None, "tp"),
            P(("grp", "dp", "kv"), None, "tp"),
            P(("grp", "dp", "kv"), None, "tp"),
            P(("grp", "dp", "kv"), None, "tp"),
            P("tp"),
            P("tp"),
            P(("grp", "dp", "kv"), None, "tp"),
            P(("grp", "dp", "kv"), None, "tp"),
            P(("grp", "dp", "kv"), None, "tp"),
            P(("grp", "dp", "kv")),
            P(("grp", "dp", "kv"), "tp", None, None),
            P("tp"),
            P("tp", "kv"),
            P(("kv", "tp")),
            P(("kv", "tp"), "dp"),
            P("dp", ("kv", "tp")),
        ),
        out_specs=P(("grp", "dp"), ("kv", "tp")),
        check_vma=False,
    )
```

profile of v0, /device:TPU:0, one launch (start us, length us, event | category | flops | bytes accessed | tf_op | source)
XLA Modules:
  0.0 172.6 jit_solution(11683976073686166705)
XLA Ops:
  6.5 1.6 copy-done
  8.1 1.3 convolution_dynamic-update-slice_fusion.1
  12.3 14.1 %all-reduce.1 = f32[8]{0:T(128)} all-reduce(f32[8]{0:T(128)S(1)} %multiply_reduce_fusion.1), channel_id=3, replica_groups=mesh['grp'=2,'dp'=2,'kv'=4,'tp'=2] {'kv'}, use_global_device_ids=true, to_apply=%region_2.0.clone | all-reduce | flops 8 | bytes 64
  29.5 1.3 compare_convert_fusion
  30.8 1.2 exponential_negate_fusion
  32.0 2.0 %copy.35 = bf16[2,128,1024]{1,2,0:T(8,128)(2,1)} copy(bf16[2,128,1024]{2,1,0:T(8,128)(2,1)} %param.40) | data formatting | bytes 1048576 | tf_op args[15]
  34.0 1.5 fusion.24
  35.5 1.3 dynamic-slice
  37.4 1.9 %fusion.22 = (f32[2,16]{1,0:T(2,128)}, f32[2,128,16]{2,1,0:T(8,128)}) fusion(f32[2,128,16]{2,1,0:T(8,128)S(1)} %copy.32, f32[2,128]{1,0:T(2,128)} %compare_convert_fusion), kind=kLoop, calls=%fused_computation.64 | loop fusion | flops 8160 | bytes 33920 | tf_op jit(solution)/shard_map/reduce_sum | solution.py:77
  39.3 1.7 reduce_window_sum.11
  41.0 1.3 fusion.19
  42.3 7.1 %all-reduce.4.cloned.1.call-done = f32[8,3088]{1,0:T(8,128)} async-done(((f32[8,3088]{1,0:T(8,128)}), f32[8,3088]{1,0:T(8,128)}) %all-reduce.4.cloned.1.call-update) | async-done | bytes 98832
  49.4 1.5 fusion.23
  50.9 1.3 reshape.87
  52.2 1.3 reshape.88
  54.9 1.3 reshape.89
  56.2 1.3 reshape.111
  62.1 1.4 fusion.28
  64.2 1.7 %fusion.29 = f32[2,16,1,64]{3,2,1,0:T(1,128)S(1)} fusion(f32[2,16,128,1]{2,3,1,0:T(1,128)S(1)} %bitcast.82, f32[2,16,64,128]{3,2,1,0:T(8,128)S(1)} %copy-done.4), kind=kOutput, calls=%fused_computation.71 | convolution fusion | flops 3145728 | bytes 1073152 | tf_op jit(solution)/shard_map/bhpn,bhn->bhp/dot_general | solution.py:94
  67.1 2.5 %psum.14 = f32[2]{0:T(128)S(1)} all-reduce(f32[2]{0:T(128)S(1)} %get-tuple-element.7), channel_id=1, replica_groups=mesh['grp'=2,'dp'=2,'kv'=4,'tp'=2] {'tp'}, use_global_device_ids=true, to_apply=%region_7.8 | all-reduce | flops 2 | bytes 16 | tf_op jit(solution)/shard_map/psum | solution.py:99
  69.6 13.2 %all-gather = bf16[4,2,1024]{2,1,0:T(2,128)(2,1)S(1)} all-gather(bf16[1,2,1024]{2,1,0:T(2,128)(2,1)S(1)} %fusion.16), channel_id=1, replica_groups=mesh['grp'=2,'dp'=2,'kv'=4,'tp'=2] {'kv'}, dimensions={0}, use_global_device_ids=true | all-gather | bytes 20480 | tf_op jit(solution)/shard_map/all_gather | solution.py:104
  82.8 2.6 %fusion.30 = f32[8,1024]{1,0:T(8,128)} fusion(bf16[8,1024]{1,0:T(8,128)(2,1)S(1)} %reshape.103, bf16[1024,1024]{1,0:T(8,128)(2,1)} %param.46), kind=kOutput, calls=%fused_computation.72 | convolution fusion | flops 16777216 | bytes 2146304 | tf_op jit(solution)/shard_map/dot_general | solution.py:103
  85.5 7.6 %reduce-scatter.4.cloned.1.call-done = f32[8,512]{1,0:T(8,128)} async-done(((f32[8,1024]{1,0:T(8,128)}), f32[8,512]{1,0:T(8,128)}) %reduce-scatter.4.cloned.1.call-update) | async-done | bytes 16400 | tf_op jit(solution)/shard_map/reduce_scatter | solution.py:106
  93.9 4.3 %all_gather.13 = bf16[16,512]{1,0:T(8,128)(2,1)S(1)} all-gather(bf16[8,512]{1,0:T(8,128)(2,1)S(1)} %get-tuple-element.5), channel_id=1, replica_groups=mesh['grp'=2,'dp'=2,'kv'=4,'tp'=2] {'dp'}, dimensions={0}, use_global_device_ids=true | all-gather | bytes 24576 | tf_op jit(solution)/shard_map/all_gather | solution.py:114
  98.2 5.4 %fusion.31 = f32[16,8192]{1,0:T(8,128)} fusion(bf16[16,512]{1,0:T(8,128)(2,1)S(1)} %all_gather.13, bf16[512,8192]{1,0:T(8,128)(2,1)} %param.48), kind=kOutput, calls=%fused_computation.73 | convolution fusion | flops 134217728 | bytes 8929280 | tf_op jit(solution)/shard_map/dot_general | solution.py:119
  103.7 4.4 %all_gather.14 = bf16[16,512]{1,0:T(8,128)(2,1)S(1)} all-gather(bf16[8,512]{1,0:T(8,128)(2,1)S(1)} %get-tuple-element.6), channel_id=1, replica_groups=mesh['grp'=2,'dp'=2,'kv'=4,'tp'=2] {'dp'}, dimensions={0}, use_global_device_ids=true | all-gather | bytes 24576 | tf_op jit(solution)/shard_map/all_gather | solution.py:115
  108.1 14.8 %psum.15 = f32[16]{0:T(128)S(1)} all-reduce(f32[16]{0:T(128)S(1)} %multiply_reduce_fusion), channel_id=1, replica_groups=mesh['grp'=2,'dp'=2,'kv'=4,'tp'=2] {'kv','tp'}, use_global_device_ids=true, to_apply=%region_11.12 | all-reduce | flops 16 | bytes 128 | tf_op jit(solution)/shard_map/psum | solution.py:120
  123.0 13.2 %reduce-scatter.6.cloned.1.call-done = f32[16,1024]{1,0:T(8,128)} async-done(((f32[16,8192]{1,0:T(8,128)}), f32[16,1024]{1,0:T(8,128)}) %reduce-scatter.6.cloned.1.call-update) | async-done | bytes 65552 | tf_op jit(solution)/shard_map/reduce_scatter | solution.py:121
  137.1 14.2 %all_gather.15 = bf16[16,8192]{1,0:T(8,128)(2,1)S(1)} all-gather(bf16[16,1024]{1,0:T(8,128)(2,1)S(1)} %multiply_convert_fusion.1), channel_id=1, replica_groups=mesh['grp'=2,'dp'=2,'kv'=4,'tp'=2] {'kv','tp'}, dimensions={1}, use_global_device_ids=true | all-gather | bytes 294912 | tf_op jit(solution)/shard_map/all_gather | solution.py:125
  151.3 5.2 %fusion.32 = f32[16,512]{1,0:T(8,128)} fusion(bf16[16,8192]{1,0:T(8,128)(2,1)S(1)} %all_gather.15, bf16[8192,512]{1,0:T(8,128)(2,1)} %param.49), kind=kOutput, calls=%fused_computation.74 | convolution fusion | flops 134217728 | bytes 8683520 | tf_op jit(solution)/shard_map/dot_general | solution.py:127
  156.5 8.3 %reduce-scatter.8.cloned.1.call-done = f32[8,512]{1,0:T(8,128)} async-done(((f32[16,512]{1,0:T(8,128)}), f32[8,512]{1,0:T(8,128)}) %reduce-scatter.8.cloned.1.call-update) | async-done | bytes 16400 | tf_op jit(solution)/shard_map/reduce_scatter | solution.py:126
  164.8 1.3 fusion.2
  (67 shorter events, 15.8 us)
Async XLA Ops:
  6.5 1.6 copy-start
  6.5 2.9 %copy-start.5 = (bf16[8,1024]{1,0:T(8,128)(2,1)S(1)}, bf16[8,1024]{1,0:T(8,128)(2,1)}, u32[]{:S(2)}) copy-start(bf16[8,1024]{1,0:T(8,128)(2,1)} %param.25) | copy-start | bytes 49156
  6.5 2.9 %copy-start.7 = (f32[1024]{0:T(1024)S(1)}, f32[1024]{0:T(1024)}, u32[]{:S(2)}) copy-start(f32[1024]{0:T(1024)} %param.26) | copy-start | bytes 12292
  6.5 42.8 %all-reduce.4.cloned.1.call-start = ((), (), s32[]{:S(2)}) async-start(), calls=%async_computation.6 | async-start | bytes 204800
  8.1 1.6 copy-start.1
  8.1 2.0 %copy-start.2 = (bf16[1024,512]{1,0:T(8,128)(2,1)S(1)}, bf16[1024,512]{1,0:T(8,128)(2,1)}, u32[]{:S(2)}) copy-start(bf16[1024,512]{1,0:T(8,128)(2,1)} %param.29) | copy-start | bytes 3145732
  9.8 1.3 copy-start.3
  9.8 1.5 copy-start.8
  9.8 16.6 %copy-start.10 = (f32[4,512]{1,0:T(4,128)S(1)}, f32[4,512]{1,0:T(4,128)}, u32[]{:S(2)}) copy-start(f32[4,512]{1,0:T(4,128)} %param.34) | copy-start | bytes 24580
  9.8 17.3 %copy-start.11 = (f32[4,512]{1,0:T(4,128)S(1)}, f32[4,512]{1,0:T(4,128)}, u32[]{:S(2)}) copy-start(f32[4,512]{1,0:T(4,128)} %param.33) | copy-start | bytes 24580
  11.4 0.6 copy-start.6
  12.1 52.1 %copy-start.4 = (f32[2,16,64,128]{3,2,1,0:T(8,128)S(1)}, f32[2,16,64,128]{3,2,1,0:T(8,128)}, u32[]{:S(2)}) copy-start(f32[2,16,64,128]{3,2,1,0:T(8,128)} %param.44) | copy-start | bytes 3145732
  12.1 81.0 %reduce-scatter.4.cloned.1.call-start = ((), (), s32[]{:S(2)}) async-start(), calls=%async_computation.3 | async-start | bytes 49152 | tf_op jit(solution)/shard_map/reduce_scatter | solution.py:106
  58.3 7.7 %copy-start.9 = (f32[2]{0:T(128)S(1)}, f32[2]{0:T(128)}, u32[]{:S(2)}) copy-start(f32[2]{0:T(128)} %fusion.19) | copy-start | bytes 28
  58.3 11.2 %copy-start.12 = (f32[1024]{0:T(1024)S(1)}, f32[1024]{0:T(1024)}, u32[]{:S(2)}) copy-start(f32[1024]{0:T(1024)} %param.45) | copy-start | bytes 12292
  61.1 32.1 %copy-start.13 = (f32[512]{0:T(512)S(1)}, f32[512]{0:T(512)}, u32[]{:S(2)}) copy-start(f32[512]{0:T(512)} %param.47) | copy-start | bytes 6148
  85.5 50.8 %reduce-scatter.6.cloned.1.call-start = ((), (), s32[]{:S(2)}) async-start(), calls=%async_computation.4 | async-start | bytes 589824 | tf_op jit(solution)/shard_map/reduce_scatter | solution.py:121
  103.6 61.2 %reduce-scatter.8.cloned.1.call-start = ((), (), s32[]{:S(2)}) async-start(), calls=%async_computation.5 | async-start | bytes 49152 | tf_op jit(solution)/shard_map/reduce_scatter | solution.py:126
Sparse Core Ops, SparseCore 0:
  12.2 37.1 all-reduce.3
  85.6 7.5 reduce-scatter.3
  103.7 32.4 reduce-scatter.5
  156.6 8.0 reduce-scatter.7
where the time goes:
time: 174 us; the launch traced here: 173 us
  blocking collectives  67.6 us (39%)
  waiting for transfers between devices  36.2 us (21%)
  matrix products  19.4 us (11%)
  local copies, waits for them, and re-layouts  18.1 us (10%)
  other arithmetic  17.4 us (10%)
  between operations  13.9 us (8%)
    psum x1, blocking collectives, per_device(): sq_sum = lax.psum(row_sq, ('kv', 'tp'))  14.8 us
    all_gather x1, blocking collectives, per_device(): hidden_units = lax.all_gather(unit_share, ('kv', 'tp'), axis=1, tiled=True)  14.2 us
    unnamed x1, blocking collectives  14.1 us
    all_gather x1, blocking collectives, per_device(): lax.all_gather(normed, 'kv', axis=0, tiled=True)  13.2 us
    reduce_scatter x1, waiting for transfers between devices, per_device(): lax.psum_scatter(partial_value, ('kv', 'tp'), scatter_dimension=1, tiled=...  13.2 us
    reduce_scatter x1, waiting for transfers between devices, per_device(): lax.psum_scatter(jnp.dot(hidden_units, w_down, preferred_element_type=jnp...  8.27 us
    reduce_scatter x1, waiting for transfers between devices, per_device(): mixed_in = lax.psum_scatter(products, 'tp', scatter_dimension=1, tiled=True)  7.61 us
    unnamed x32, local copies, waits for them, and re-layouts  7.41 us
  transfers between devices with their start and end apart: 4, of which 4 were waited for; matrix products, arithmetic and copies ran while one was open for 9% of the time, Pallas kernels for 0%

commit v1 on v0

--- a/solution.py
+++ b/solution.py
@@ -122,7 +122,7 @@
     unit_share = jnp.square(jax.nn.relu(shares * lax.rsqrt(sq_sum / D + EPS)[:, None])).astype(
         jnp.bfloat16
     )
-    hidden_units = lax.all_gather(unit_share, ("kv", "tp"), axis=1, tiled=True)
+    hidden_units = jnp.concatenate(lax.all_gather(unit_share, ("kv", "tp")), axis=1)
     lowered = lax.psum_scatter(
         jnp.dot(hidden_units, w_down, preferred_element_type=jnp.float32),
         "dp",

time: 174 us -> 174 us (level)
    unnamed x32 -> x33, local copies, waits for them, and re-layouts: 7.41 us -> 7.43 us
where the time goes in v1:
time: 174 us; the launch traced here: 173 us
  blocking collectives  67.6 us (39%)
  waiting for transfers between devices  36.2 us (21%)
  matrix products  19.4 us (11%)
  local copies, waits for them, and re-layouts  18.1 us (10%)
  other arithmetic  17.4 us (10%)
  between operations  13.9 us (8%)
    psum x1, blocking collectives, per_device(): sq_sum = lax.psum(row_sq, ('kv', 'tp'))  14.8 us
    all_gather x1, blocking collectives, per_device(): lax.all_gather(unit_share, ('kv', 'tp'))  14.2 us
    unnamed x1, blocking collectives  14.1 us
    all_gather x1, blocking collectives, per_device(): lax.all_gather(normed, 'kv', axis=0, tiled=True)  13.2 us
    reduce_scatter x1, waiting for transfers between devices, per_device(): lax.psum_scatter(partial_value, ('kv', 'tp'), scatter_dimension=1, tiled=...  13.2 us
    reduce_scatter x1, waiting for transfers between devices, per_device(): lax.psum_scatter(jnp.dot(hidden_units, w_down, preferred_element_type=jnp...  8.27 us
    reduce_scatter x1, waiting for transfers between devices, per_device(): mixed_in = lax.psum_scatter(products, 'tp', scatter_dimension=1, tiled=True)  7.61 us
    unnamed x33, local copies, waits for them, and re-layouts  7.43 us
  transfers between devices with their start and end apart: 4, of which 4 were waited for; matrix products, arithmetic and copies ran while one was open for 9% of the time, Pallas kernels for 0%

profile of v1, /device:TPU:0, one launch (start us, length us, event | category | flops | bytes accessed | tf_op | source)
XLA Modules:
  0.0 172.7 jit_solution(7608849386855593714)
XLA Ops:
  6.5 1.6 copy-done
  8.1 1.3 convolution_dynamic-update-slice_fusion.1
  12.3 14.1 %all-reduce.1 = f32[8]{0:T(128)} all-reduce(f32[8]{0:T(128)S(1)} %multiply_reduce_fusion.1), channel_id=4, replica_groups=mesh['grp'=2,'dp'=2,'kv'=4,'tp'=2] {'kv'}, use_global_device_ids=true, to_apply=%region_2.0.clone | all-reduce | flops 8 | bytes 64
  29.5 1.3 compare_convert_fusion
  30.8 1.2 exponential_negate_fusion
  32.0 2.0 %copy.36 = bf16[2,128,1024]{1,2,0:T(8,128)(2,1)} copy(bf16[2,128,1024]{2,1,0:T(8,128)(2,1)} %param.40) | data formatting | bytes 1048576 | tf_op args[15]
  34.0 1.5 fusion.24
  35.5 1.3 dynamic-slice
  37.4 1.9 %fusion.22 = (f32[2,16]{1,0:T(2,128)}, f32[2,128,16]{2,1,0:T(8,128)}) fusion(f32[2,128,16]{2,1,0:T(8,128)S(1)} %copy.33, f32[2,128]{1,0:T(2,128)} %compare_convert_fusion), kind=kLoop, calls=%fused_computation.64 | loop fusion | flops 8160 | bytes 33920 | tf_op jit(solution)/shard_map/reduce_sum | solution.py:77
  39.3 1.7 reduce_window_sum.11
  41.0 1.3 fusion.19
  42.3 7.1 %all-reduce.4.cloned.1.call-done = f32[8,3088]{1,0:T(8,128)} async-done(((f32[8,3088]{1,0:T(8,128)}), f32[8,3088]{1,0:T(8,128)}) %all-reduce.4.cloned.1.call-update) | async-done | bytes 98832
  49.4 1.5 fusion.23
  50.9 1.3 reshape.93
  52.2 1.3 reshape.94
  54.9 1.3 reshape.95
  56.2 1.3 reshape.120
  62.1 1.4 fusion.28
  64.2 1.7 %fusion.29 = f32[2,16,1,64]{3,2,1,0:T(1,128)S(1)} fusion(f32[2,16,128,1]{2,3,1,0:T(1,128)S(1)} %bitcast.90, f32[2,16,64,128]{3,2,1,0:T(8,128)S(1)} %copy-done.4), kind=kOutput, calls=%fused_computation.71 | convolution fusion | flops 3145728 | bytes 1073152 | tf_op jit(solution)/shard_map/bhpn,bhn->bhp/dot_general | solution.py:94
  67.1 2.5 %psum.14 = f32[2]{0:T(128)S(1)} all-reduce(f32[2]{0:T(128)S(1)} %get-tuple-element.7), channel_id=1, replica_groups=mesh['grp'=2,'dp'=2,'kv'=4,'tp'=2] {'tp'}, use_global_device_ids=true, to_apply=%region_7.8 | all-reduce | flops 2 | bytes 16 | tf_op jit(solution)/shard_map/psum | solution.py:99
  69.6 13.2 %all-gather.1 = bf16[4,2,1024]{2,1,0:T(2,128)(2,1)S(1)} all-gather(bf16[1,2,1024]{2,1,0:T(2,128)(2,1)S(1)} %fusion.16), channel_id=1, replica_groups=mesh['grp'=2,'dp'=2,'kv'=4,'tp'=2] {'kv'}, dimensions={0}, use_global_device_ids=true | all-gather | bytes 20480 | tf_op jit(solution)/shard_map/all_gather | solution.py:104
  82.8 2.6 %fusion.30 = f32[8,1024]{1,0:T(8,128)} fusion(bf16[8,1024]{1,0:T(8,128)(2,1)S(1)} %reshape.112, bf16[1024,1024]{1,0:T(8,128)(2,1)} %param.46), kind=kOutput, calls=%fused_computation.72 | convolution fusion | flops 16777216 | bytes 2146304 | tf_op jit(solution)/shard_map/dot_general | solution.py:103
  85.5 7.6 %reduce-scatter.4.cloned.1.call-done = f32[8,512]{1,0:T(8,128)} async-done(((f32[8,1024]{1,0:T(8,128)}), f32[8,512]{1,0:T(8,128)}) %reduce-scatter.4.cloned.1.call-update) | async-done | bytes 16400 | tf_op jit(solution)/shard_map/reduce_scatter | solution.py:106
  93.9 4.3 %all_gather.16 = bf16[16,512]{1,0:T(8,128)(2,1)S(1)} all-gather(bf16[8,512]{1,0:T(8,128)(2,1)S(1)} %get-tuple-element.5), channel_id=1, replica_groups=mesh['grp'=2,'dp'=2,'kv'=4,'tp'=2] {'dp'}, dimensions={0}, use_global_device_ids=true | all-gather | bytes 24576 | tf_op jit(solution)/shard_map/all_gather | solution.py:114
  98.2 5.4 %fusion.31 = f32[16,8192]{1,0:T(8,128)} fusion(bf16[16,512]{1,0:T(8,128)(2,1)S(1)} %all_gather.16, bf16[512,8192]{1,0:T(8,128)(2,1)} %param.48), kind=kOutput, calls=%fused_computation.73 | convolution fusion | flops 134217728 | bytes 8929280 | tf_op jit(solution)/shard_map/dot_general | solution.py:119
  103.7 4.4 %all_gather.17 = bf16[16,512]{1,0:T(8,128)(2,1)S(1)} all-gather(bf16[8,512]{1,0:T(8,128)(2,1)S(1)} %get-tuple-element.6), channel_id=1, replica_groups=mesh['grp'=2,'dp'=2,'kv'=4,'tp'=2] {'dp'}, dimensions={0}, use_global_device_ids=true | all-gather | bytes 24576 | tf_op jit(solution)/shard_map/all_gather | solution.py:115
  108.1 14.8 %psum.15 = f32[16]{0:T(128)S(1)} all-reduce(f32[16]{0:T(128)S(1)} %multiply_reduce_fusion), channel_id=1, replica_groups=mesh['grp'=2,'dp'=2,'kv'=4,'tp'=2] {'kv','tp'}, use_global_device_ids=true, to_apply=%region_11.12 | all-reduce | flops 16 | bytes 128 | tf_op jit(solution)/shard_map/psum | solution.py:120
  123.0 13.2 %reduce-scatter.6.cloned.1.call-done = f32[16,1024]{1,0:T(8,128)} async-done(((f32[16,8192]{1,0:T(8,128)}), f32[16,1024]{1,0:T(8,128)}) %reduce-scatter.6.cloned.1.call-update) | async-done | bytes 65552 | tf_op jit(solution)/shard_map/reduce_scatter | solution.py:121
  137.1 14.2 %all-gather = bf16[128,1024]{1,0:T(8,128)(2,1)S(1)} all-gather(bf16[16,1024]{1,0:T(8,128)(2,1)S(1)} %multiply_convert_fusion.1), channel_id=2, replica_groups=mesh['grp'=2,'dp'=2,'kv'=4,'tp'=2] {'kv','tp'}, dimensions={0}, use_global_device_ids=true | all-gather | bytes 294912 | tf_op jit(solution)/shard_map/all_gather | solution.py:125
  151.3 5.2 %fusion.32 = f32[16,512]{1,0:T(8,128)} fusion(bf16[16,8192]{1,0:T(8,128)(2,1)S(1)} %bitcast.86, bf16[8192,512]{1,0:T(8,128)(2,1)} %param.49), kind=kOutput, calls=%fused_computation.74 | convolution fusion | flops 134217728 | bytes 8683520 | tf_op jit(solution)/shard_map/dot_general | solution.py:127
  156.5 8.3 %reduce-scatter.8.cloned.1.call-done = f32[8,512]{1,0:T(8,128)} async-done(((f32[16,512]{1,0:T(8,128)}), f32[8,512]{1,0:T(8,128)}) %reduce-scatter.8.cloned.1.call-update) | async-done | bytes 16400 | tf_op jit(solution)/shard_map/reduce_scatter | solution.py:126
  164.8 1.3 fusion.2
  (68 shorter events, 15.8 us)
Async XLA Ops:
  6.5 1.6 copy-start
  6.5 2.9 %copy-start.5 = (bf16[8,1024]{1,0:T(8,128)(2,1)S(1)}, bf16[8,1024]{1,0:T(8,128)(2,1)}, u32[]{:S(2)}) copy-start(bf16[8,1024]{1,0:T(8,128)(2,1)} %param.25) | copy-start | bytes 49156
  6.5 2.9 %copy-start.7 = (f32[1024]{0:T(1024)S(1)}, f32[1024]{0:T(1024)}, u32[]{:S(2)}) copy-start(f32[1024]{0:T(1024)} %param.26) | copy-start | bytes 12292
  6.5 42.8 %all-reduce.4.cloned.1.call-start = ((), (), s32[]{:S(2)}) async-start(), calls=%async_computation.6 | async-start | bytes 204800
  8.1 1.6 copy-start.1
  8.1 2.0 %copy-start.2 = (bf16[1024,512]{1,0:T(8,128)(2,1)S(1)}, bf16[1024,512]{1,0:T(8,128)(2,1)}, u32[]{:S(2)}) copy-start(bf16[1024,512]{1,0:T(8,128)(2,1)} %param.29) | copy-start | bytes 3145732
  9.8 1.3 copy-start.3
  9.8 1.5 copy-start.8
  9.8 16.6 %copy-start.10 = (f32[4,512]{1,0:T(4,128)S(1)}, f32[4,512]{1,0:T(4,128)}, u32[]{:S(2)}) copy-start(f32[4,512]{1,0:T(4,128)} %param.34) | copy-start | bytes 24580
  9.8 17.3 %copy-start.11 = (f32[4,512]{1,0:T(4,128)S(1)}, f32[4,512]{1,0:T(4,128)}, u32[]{:S(2)}) copy-start(f32[4,512]{1,0:T(4,128)} %param.33) | copy-start | bytes 24580
  11.4 0.6 copy-start.6
  12.1 52.1 %copy-start.4 = (f32[2,16,64,128]{3,2,1,0:T(8,128)S(1)}, f32[2,16,64,128]{3,2,1,0:T(8,128)}, u32[]{:S(2)}) copy-start(f32[2,16,64,128]{3,2,1,0:T(8,128)} %param.44) | copy-start | bytes 3145732
  12.1 81.0 %reduce-scatter.4.cloned.1.call-start = ((), (), s32[]{:S(2)}) async-start(), calls=%async_computation.3 | async-start | bytes 49152 | tf_op jit(solution)/shard_map/reduce_scatter | solution.py:106
  58.3 7.7 %copy-start.9 = (f32[2]{0:T(128)S(1)}, f32[2]{0:T(128)}, u32[]{:S(2)}) copy-start(f32[2]{0:T(128)} %fusion.19) | copy-start | bytes 28
  58.3 11.2 %copy-start.12 = (f32[1024]{0:T(1024)S(1)}, f32[1024]{0:T(1024)}, u32[]{:S(2)}) copy-start(f32[1024]{0:T(1024)} %param.45) | copy-start | bytes 12292
  61.1 32.1 %copy-start.13 = (f32[512]{0:T(512)S(1)}, f32[512]{0:T(512)}, u32[]{:S(2)}) copy-start(f32[512]{0:T(512)} %param.47) | copy-start | bytes 6148
  85.5 50.8 %reduce-scatter.6.cloned.1.call-start = ((), (), s32[]{:S(2)}) async-start(), calls=%async_computation.4 | async-start | bytes 589824 | tf_op jit(solution)/shard_map/reduce_scatter | solution.py:121
  103.6 61.2 %reduce-scatter.8.cloned.1.call-start = ((), (), s32[]{:S(2)}) async-start(), calls=%async_computation.5 | async-start | bytes 49152 | tf_op jit(solution)/shard_map/reduce_scatter | solution.py:126
Sparse Core Ops, SparseCore 0:
  12.2 37.1 all-reduce.3
  85.6 7.5 reduce-scatter.3
  103.7 32.4 reduce-scatter.5
  156.7 8.0 reduce-scatter.7
